TPU v7x, 512 devices: a whole 4x8x8 slice. The times are simulated.
512 devices in a mesh: fs: 64 (over z, y), tp: 8 (over x, core).
Axes of the slice: x: 4, y: 8, z: 8, core: 2. Of those that a mesh axis runs over, the one named last changes fastest.
Arguments:
- saved_input: bfloat16 [65536, 2048], P('fs'), may hold values from -60 to 60
- out_cotangent: bfloat16 [65536, 4096], P('fs', 'tp'), may hold values from -6 to 6
- old_weight: float32 [2048, 4096], P('fs', 'tp'), may hold values from -0.125 to 0.125
- factor: bfloat16 [4096, 256], P('tp'), may hold values from -0.09375 to 0.09375
- moment_first: float32 [2048, 256], P('fs'), may hold values from -3 to 3
- moment_second: float32 [2048, 256], P('fs'), may hold values from 0.05 to 1
Outputs:
- new_weight: float32 [2048, 4096], P('fs', 'tp')
- update: float32 [2048, 4096], P('fs', 'tp')
- new_first: float32 [2048, 256], P('fs')
- new_second: float32 [2048, 256], P('fs')
- weight_copy: bfloat16 [2048, 4096], P(None, 'tp')
All inputs are finite; a program needn't handle non-finite values.
Results may differ from a plain program's by a relative error of at most 0.0028.
Values may be sent and summed in bfloat16 or wider, within the bound.
No kernel may reach another device: no remote copies, remote signals or barrier semaphores. Data moves between devices by JAX's collectives and lax.ppermute only.
A program may use at most 64 MiB of HBM per device.

v0:
```python
import math
import jax
import jax.numpy as jnp
from jax import lax
from jax.sharding import Mesh
from jax.sharding import PartitionSpec as P

HV = 2048
RANK = 256
FS = ("fs_0", "fs_1")


def in_blocks(shard, dim, devices):
    before, after = (shard.shape[:dim], shard.shape[dim + 1 :])
    return jnp.moveaxis(shard.reshape(*before, devices, -1, *after), dim, 0)


def sent_and_summed(shard, axis, dim):
    devices = lax.axis_size(axis)
    tiles = lax.all_to_all(in_blocks(shard, dim, devices), axis, 0, 0, tiled=True)
    return jnp.sum(tiles.astype(jnp.float32), axis=0)


def copy_for_each(shard, axis):
    devices = lax.axis_size(axis)
    return lax.all_to_all(
        jnp.broadcast_to(shard[None], (devices, *shard.shape)), axis, 0, 0, tiled=True
    )


def taken_together(shard, axis):
    return copy_for_each(shard, axis).sum(axis=0)


def one_axis_at_a_time(shard, axes):
    for axis in axes:
        shard = lax.psum(shard, axis)
    return shard


def laid_out(tiles, dim):
    tiles = jnp.moveaxis(tiles, 0, dim)
    dims = tiles.shape
    return tiles.reshape(*dims[:dim], dims[dim] * dims[dim + 1], *dims[dim + 2 :])


def stacked_from(shard, axes, order):
    tiles = shard[None]
    for k in order:
        tiles = lax.all_gather(tiles, axes[k], axis=0, tiled=True)
    held = [lax.axis_size(axes[k]) for k in reversed(order)]
    tiles = tiles.reshape(*held, *shard.shape)
    turned = sorted(range(len(order)), key=lambda place: order[len(order) - 1 - place])
    return tiles.transpose(*turned, *range(len(order), tiles.ndim)).reshape(-1, *shard.shape)


def whole_of(shard, axes, order, dim):
    return laid_out(stacked_from(shard, axes, order), dim)


def on_device(saved_input, out_cotangent, old_weight, factor, moment_first, moment_second):
    wide_factor = factor.astype(jnp.float32)
    contract = (((0,), (0,)), ((), ()))
    gradient = sent_and_summed(
        lax.dot_general(
            saved_input, out_cotangent, contract, preferred_element_type=jnp.float32
        ).astype(jnp.bfloat16),
        FS,
        0,
    )
    partial_low = jnp.dot(gradient, wide_factor, precision=lax.Precision.HIGHEST)
    projected = taken_together(partial_low, "tp")
    squares = one_axis_at_a_time(jnp.sum(projected * projected), FS)
    clip = jnp.minimum(1.0, math.sqrt(HV * RANK) / (jnp.sqrt(squares) + 1e-06))
    clipped = clip * projected
    new_first = 0.9 * moment_first + 0.1 * clipped
    new_second = 0.95 * moment_second + 0.05 * clipped * clipped
    direction = new_first / (jnp.sqrt(new_second) + 1e-08)
    update = jnp.dot(direction, wide_factor.T, precision=lax.Precision.HIGHEST)
    new_weight = old_weight - 0.05 * update
    copied = whole_of(new_weight.astype(jnp.bfloat16), FS, (0, 1), 0)
    return (new_weight, update, new_first, new_second, copied)


def solution(mesh):
    finer = Mesh(mesh.devices.reshape(8, 8, mesh.shape["tp"]), ("fs_0", "fs_1", "tp"))
    in_specs = (P(FS, None), P(FS, "tp"), P(FS, "tp"), P("tp", None), P(FS, None), P(FS, None))
    out_specs = (P(FS, "tp"), P(FS, "tp"), P(FS, None), P(FS, None), P(None, "tp"))
    return jax.shard_map(
        on_device, mesh=finer, in_specs=in_specs, out_specs=out_specs, check_vma=False
    )
```

profile of v0, /device:TPU:2, one launch (start us, length us, event | category | flops | bytes accessed | tf_op | source)
XLA Modules:
  0.0 204.9 jit_solution(14049241271818606529)
XLA Ops:
  7.2 0.0 copy-start
  7.2 0.0 all-gather.3.cloned.1.call-start
  7.2 1.2 copy-done
  8.4 4.6 %convolution_convert_fusion = bf16[2048,512]{1,0:T(8,128)(2,1)S(1)} fusion(bf16[1024,2048]{1,0:T(8,128)(2,1)} %param.6, bf16[1024,512]{1,0:T(8,128)(2,1)S(1)} %copy-done), kind=kOutput, calls=%fused_computation.1 | convolution fusion | flops 2148532224 | bytes 7340032 | tf_op jit(solution)/shard_map/dot_general | solution.py:65
  13.0 0.0 copy-start.1
  13.0 0.0 copy-start.5
  13.0 0.0 copy-start.6
  13.0 0.0 copy-start.4
  13.0 68.7 %all_to_all.10 = bf16[64,32,512]{2,1,0:T(8,128)(2,1)S(1)} all-to-all(bf16[64,32,512]{2,1,0:T(8,128)(2,1)S(1)} %bitcast.13), channel_id=1, replica_groups=mesh['fs_0'=8,'fs_1'=8,'tp'=8] {'fs_0','fs_1'}, dimensions={0} | all-to-all | bytes 4194304 | tf_op jit(solution)/shard_map/all_to_all | solution.py:20
  81.7 0.3 convert_reduce_fusion
  82.0 0.0 copy-done.1
  82.0 0.2 fusion.8
  82.3 10.7 %all_to_all.11 = f32[8,32,256]{2,1,0:T(8,128)S(1)} all-to-all(f32[8,32,256]{2,1,0:T(8,128)S(1)} %broadcast_in_dim.4), channel_id=1, replica_groups=mesh['fs_0'=8,'fs_1'=8,'tp'=8] {'tp'}, dimensions={0} | all-to-all | bytes 524288 | tf_op jit(solution)/shard_map/all_to_all | solution.py:26
  93.0 0.6 multiply_reduce_fusion
  93.6 16.6 %psum.14 = f32[]{:T(128)} all-reduce(f32[]{:T(128)} %multiply_reduce_fusion), channel_id=1, replica_groups=mesh['fs_0'=8,'fs_1'=8,'tp'=8] {'fs_0'}, use_global_device_ids=true, to_apply=%region_3.0 | all-reduce | flops 1 | bytes 8 | tf_op jit(solution)/shard_map/psum | solution.py:37
  110.2 16.5 %psum.15 = f32[]{:T(128)} all-reduce(f32[]{:T(128)} %psum.14), channel_id=1, replica_groups=mesh['fs_0'=8,'fs_1'=8,'tp'=8] {'fs_1'}, use_global_device_ids=true, to_apply=%region_4.0 | all-reduce | flops 1 | bytes 8 | tf_op jit(solution)/shard_map/psum | solution.py:37
  127.5 0.0 copy-done.5
  127.5 0.0 copy-done.6
  127.5 0.0 copy-start.2
  127.5 0.0 copy-start.3
  127.5 0.0 copy-done.4
  127.5 1.0 fusion.7
  128.5 26.8 %all-gather = bf16[256,512]{1,0:T(8,128)(2,1)} all-gather(bf16[32,512]{1,0:T(8,128)(2,1)S(1)} %get-tuple-element.5), channel_id=2, replica_groups=mesh['fs_0'=8,'fs_1'=8,'tp'=8] {'fs_0'}, dimensions={0}, use_global_device_ids=true | all-gather | bytes 294912 | tf_op jit(solution)/shard_map/all_gather | solution.py:50
  155.4 0.0 all-gather.3.cloned.1.call-update
  155.4 39.5 %all-gather.3.cloned.1.call-done = bf16[64,32,512]{2,1,0:T(8,128)(2,1)} async-done(((bf16[8,32,512]{2,1,0:T(8,128)(2,1)}), bf16[64,32,512]{2,1,0:T(8,128)(2,1)}) %all-gather.3.cloned.1.call-update) | async-done | bytes 2097168 | tf_op jit(solution)/shard_map/all_gather | solution.py:50
  194.9 3.2 %copy.13 = bf16[8,8,32,512]{3,2,1,0:T(8,128)(2,1)} copy(bf16[8,8,32,512]{3,2,0,1:T(8,128)(2,1)} %bitcast.12) | data formatting | bytes 4194304 | tf_op jit(solution)/shard_map/transpose | solution.py:54
  198.1 0.0 copy-done.2
  198.1 0.0 copy-done.3
  (3 shorter events, 0.1 us)
Async XLA Ops:
  7.2 1.2 copy-start
  7.2 187.7 %all-gather.3.cloned.1.call-start = ((), (), s32[]{:S(2)}) async-start(), calls=%async_computation.2 | async-start | bytes 2359296 | tf_op jit(solution)/shard_map/all_gather | solution.py:50
  13.0 69.1 %copy-start.1 = (bf16[512,256]{1,0:T(8,128)(2,1)S(1)}, bf16[512,256]{1,0:T(8,128)(2,1)}, u32[]{:S(2)}) copy-start(bf16[512,256]{1,0:T(8,128)(2,1)} %param.9) | copy-start | bytes 786436
  13.0 114.5 %copy-start.5 = (f32[32,256]{1,0:T(8,128)S(1)}, f32[32,256]{1,0:T(8,128)}, u32[]{:S(2)}) copy-start(f32[32,256]{1,0:T(8,128)} %param.11) | copy-start | bytes 98308
  13.0 114.5 %copy-start.6 = (f32[32,256]{1,0:T(8,128)S(1)}, f32[32,256]{1,0:T(8,128)}, u32[]{:S(2)}) copy-start(f32[32,256]{1,0:T(8,128)} %param.10) | copy-start | bytes 98308
  13.0 114.5 %copy-start.4 = (f32[32,512]{1,0:T(8,128)S(1)}, f32[32,512]{1,0:T(8,128)}, u32[]{:S(2)}) copy-start(f32[32,512]{1,0:T(8,128)} %param.8) | copy-start | bytes 196612
  127.5 70.6 %copy-start.2 = (f32[32,256]{1,0:T(8,128)}, f32[32,256]{1,0:T(8,128)S(1)}, u32[]{:S(2)}) copy-start(f32[32,256]{1,0:T(8,128)S(1)} %get-tuple-element.7) | copy-start | bytes 98308
  127.5 70.6 %copy-start.3 = (f32[32,256]{1,0:T(8,128)}, f32[32,256]{1,0:T(8,128)S(1)}, u32[]{:S(2)}) copy-start(f32[32,256]{1,0:T(8,128)S(1)} %get-tuple-element.8) | copy-start | bytes 98308
Sparse Core Ops, SparseCore 0:
  155.5 39.3 all-gather.2
where the time goes:
time: 205 us
  blocking collectives  139 us (68%)
  waiting for transfers between devices  39.5 us (19%)
  between operations  14.9 us (7%)
  matrix products  5.81 us (3%)
  local copies, waits for them, and re-layouts  4.39 us (2%)
    all_to_all x1, blocking collectives, sent_and_summed(): lax.all_to_all(in_blocks(shard, dim, devices), axis, 0, 0, tiled=True)  68.7 us
    all_gather x1, waiting for transfers between devices, stacked_from(): tiles = lax.all_gather(tiles, axes[k], axis=0, tiled=True)  39.5 us
    psum x2, blocking collectives, one_axis_at_a_time(): shard = lax.psum(shard, axis)  33.1 us
    all_gather x1, blocking collectives, stacked_from(): tiles = lax.all_gather(tiles, axes[k], axis=0, tiled=True)  26.8 us
    all_to_all x1, blocking collectives, copy_for_each(): lax.all_to_all(jnp.broadcast_to(shard[None], (devices, *shard.shape)), ax...  10.7 us
    dot_general x1, matrix products, on_device(): lax.dot_general(saved_input, out_cotangent, contract, preferred_element_t...  4.56 us
  transfers between devices with their start and end apart: 1, of which 1 were waited for; matrix products, arithmetic and copies ran while one was open for 0% of the time, Pallas kernels for 0%

commit v1 on v0

--- a/solution.py
+++ b/solution.py
@@ -47,7 +47,9 @@
 def stacked_from(shard, axes, order):
     tiles = shard[None]
     for k in order:
-        tiles = lax.all_gather(tiles, axes[k], axis=0, tiled=True)
+        tiles = jnp.concatenate(
+            lax.all_to_all(jnp.stack([tiles] * lax.axis_size(axes[k])), axes[k], 0, 0), axis=0
+        )
     held = [lax.axis_size(axes[k]) for k in reversed(order)]
     tiles = tiles.reshape(*held, *shard.shape)
     turned = sorted(range(len(order)), key=lambda place: order[len(order) - 1 - place])

time: 205 us -> 186 us (0.907)
  waiting for transfers between devices: 39.5 us -> 0 us
  blocking collectives: 139 us -> 174 us
  between operations: 14.9 us -> 1.47 us
    all_to_all x0 -> x2, blocking collectives: none -> 61.7 us  [stacked_from(): lax.all_to_all(jnp.stack([tiles] * lax.axis_size(axes[k])), axes[k], 0, 0)]
    all_gather x1 -> x0, waiting for transfers between devices: 39.5 us -> none  [stacked_from(): tiles = lax.all_gather(tiles, axes[k], axis=0, tiled=True)]
    all_gather x1 -> x0, blocking collectives: 26.8 us -> none  [stacked_from(): tiles = lax.all_gather(tiles, axes[k], axis=0, tiled=True)]
    transpose x1 -> x0, local copies, waits for them, and re-layouts: 3.16 us -> none  [stacked_from(): tiles.transpose(*turned, *range(len(order), tiles.ndim))]
  transfers between devices with their start and end apart: 1 -> 0, of which waited for: 1 -> 0; matrix products, arithmetic and copies ran while one was open for 0% -> 0% of each run, Pallas kernels for 0% -> 0%
where the time goes in v1:
time: 186 us
  blocking collectives  174 us (94%)
  matrix products  5.81 us (3%)
  local copies, waits for them, and re-layouts  3.7 us (2%)
    all_to_all x1, blocking collectives, sent_and_summed(): lax.all_to_all(in_blocks(shard, dim, devices), axis, 0, 0, tiled=True)  68.5 us
    all_to_all x2, blocking collectives, stacked_from(): lax.all_to_all(jnp.stack([tiles] * lax.axis_size(axes[k])), axes[k], 0, 0)  61.7 us
    psum x2, blocking collectives, one_axis_at_a_time(): shard = lax.psum(shard, axis)  33.1 us
    all_to_all x1, blocking collectives, copy_for_each(): lax.all_to_all(jnp.broadcast_to(shard[None], (devices, *shard.shape)), ax...  10.7 us
    dot_general x1, matrix products, on_device(): lax.dot_general(saved_input, out_cotangent, contract, preferred_element_t...  4.56 us

profile of v1, /device:TPU:2, one launch (start us, length us, event | category | flops | bytes accessed | tf_op | source)
XLA Modules:
  0.0 186.0 jit_solution(15490089011415035420)
XLA Ops:
  0.6 0.0 copy-start
  0.6 1.2 copy-done
  1.9 4.6 %convolution_convert_fusion = bf16[2048,512]{1,0:T(8,128)(2,1)S(1)} fusion(bf16[1024,2048]{1,0:T(8,128)(2,1)} %param.6, bf16[1024,512]{1,0:T(8,128)(2,1)S(1)} %copy-done), kind=kOutput, calls=%fused_computation.1 | convolution fusion | flops 2148532224 | bytes 7340032 | tf_op jit(solution)/shard_map/dot_general | solution.py:67
  6.4 68.5 %all_to_all.20 = bf16[64,32,512]{2,1,0:T(8,128)(2,1)S(1)} all-to-all(bf16[64,32,512]{2,1,0:T(8,128)(2,1)S(1)} %bitcast.11), channel_id=1, replica_groups=mesh['fs_0'=8,'fs_1'=8,'tp'=8] {'fs_0','fs_1'}, dimensions={0} | all-to-all | bytes 4194304 | tf_op jit(solution)/shard_map/all_to_all | solution.py:20
  75.0 0.0 copy-start.1
  75.0 0.0 copy-start.5
  75.0 0.0 copy-start.6
  75.0 0.0 copy-start.4
  75.0 0.3 convert_reduce_fusion
  75.3 0.6 copy-done.1
  75.9 0.2 fusion.8
  76.2 10.7 %all_to_all.21 = f32[8,32,256]{2,1,0:T(8,128)S(1)} all-to-all(f32[8,32,256]{2,1,0:T(8,128)S(1)} %broadcast_in_dim.2), channel_id=1, replica_groups=mesh['fs_0'=8,'fs_1'=8,'tp'=8] {'tp'}, dimensions={0} | all-to-all | bytes 524288 | tf_op jit(solution)/shard_map/all_to_all | solution.py:26
  86.9 0.6 multiply_reduce_fusion
  87.5 16.6 %psum.14 = f32[]{:T(128)} all-reduce(f32[]{:T(128)} %multiply_reduce_fusion), channel_id=1, replica_groups=mesh['fs_0'=8,'fs_1'=8,'tp'=8] {'fs_0'}, use_global_device_ids=true, to_apply=%region_3.0 | all-reduce | flops 1 | bytes 8 | tf_op jit(solution)/shard_map/psum | solution.py:37
  104.1 16.5 %psum.15 = f32[]{:T(128)} all-reduce(f32[]{:T(128)} %psum.14), channel_id=1, replica_groups=mesh['fs_0'=8,'fs_1'=8,'tp'=8] {'fs_1'}, use_global_device_ids=true, to_apply=%region_4.0 | all-reduce | flops 1 | bytes 8 | tf_op jit(solution)/shard_map/psum | solution.py:37
  121.4 0.0 copy-done.5
  121.4 0.0 copy-done.6
  121.4 0.0 copy-start.2
  121.4 0.0 copy-start.3
  121.4 0.0 copy-done.4
  121.4 1.0 fusion.7
  122.5 15.2 %all_to_all.22 = bf16[8,1,32,512]{3,2,1,0:T(8,128)(2,1)S(1)} all-to-all(bf16[8,1,32,512]{3,2,1,0:T(8,128)(2,1)S(1)} %stack.6), channel_id=1, replica_groups=mesh['fs_0'=8,'fs_1'=8,'tp'=8] {'fs_0'}, dimensions={0} | all-to-all | bytes 524288 | tf_op jit(solution)/shard_map/all_to_all | solution.py:51
  137.6 0.2 stack.7
  137.9 46.6 %all_to_all.23 = bf16[8,8,32,512]{3,2,1,0:T(8,128)(2,1)S(1)} all-to-all(bf16[8,8,32,512]{3,2,1,0:T(8,128)(2,1)S(1)} %stack.7), channel_id=1, replica_groups=mesh['fs_0'=8,'fs_1'=8,'tp'=8] {'fs_1'}, dimensions={0} | all-to-all | bytes 4194304 | tf_op jit(solution)/shard_map/all_to_all | solution.py:51
  184.5 0.0 copy-done.2
  184.5 0.0 copy-done.3
  184.5 1.6 copy.12
  (4 shorter events, 0.1 us)
Async XLA Ops:
  0.6 1.2 copy-start
  75.0 1.0 copy-start.1
  75.0 46.4 %copy-start.5 = (f32[32,256]{1,0:T(8,128)S(1)}, f32[32,256]{1,0:T(8,128)}, u32[]{:S(2)}) copy-start(f32[32,256]{1,0:T(8,128)} %param.11) | copy-start | bytes 98308
  75.0 46.4 %copy-start.6 = (f32[32,256]{1,0:T(8,128)S(1)}, f32[32,256]{1,0:T(8,128)}, u32[]{:S(2)}) copy-start(f32[32,256]{1,0:T(8,128)} %param.10) | copy-start | bytes 98308
  75.0 46.4 %copy-start.4 = (f32[32,512]{1,0:T(8,128)S(1)}, f32[32,512]{1,0:T(8,128)}, u32[]{:S(2)}) copy-start(f32[32,512]{1,0:T(8,128)} %param.8) | copy-start | bytes 196612
  121.4 63.1 %copy-start.2 = (f32[32,256]{1,0:T(8,128)}, f32[32,256]{1,0:T(8,128)S(1)}, u32[]{:S(2)}) copy-start(f32[32,256]{1,0:T(8,128)S(1)} %get-tuple-element.7) | copy-start | bytes 98308
  121.4 63.1 %copy-start.3 = (f32[32,256]{1,0:T(8,128)}, f32[32,256]{1,0:T(8,128)S(1)}, u32[]{:S(2)}) copy-start(f32[32,256]{1,0:T(8,128)S(1)} %get-tuple-element.8) | copy-start | bytes 98308
